TPU v7x, 32 devices: a whole 2x2x4 slice. The times are simulated.
32 devices in a mesh: fs: 8 (over z, y), tp: 4 (over x, core).
Axes of the slice: x: 2, y: 2, z: 4, core: 2. Of those that a mesh axis runs over, the one named last changes fastest.
Arguments:
- mixed: bfloat16 [12288, 2048], P(('fs', 'tp')), may hold values from -6 to 6
- residual: bfloat16 [12288, 2048], P(('fs', 'tp')), may hold values from -6 to 6
- mix_weight: bfloat16 [2048, 2048], P(('fs', 'tp')), may hold values from -0.125 to 0.125
- norm_gain: float32 [2048], replicated, may hold values from 0.1 to 1.9
- up_weight: bfloat16 [2048, 5504], P('fs', 'tp'), may hold values from -0.125 to 0.125
- gate_weight: bfloat16 [2048, 5504], P('fs', 'tp'), may hold values from -0.125 to 0.125
- conv_weight: float32 [3, 5504], P(None, 'tp'), may hold values from -3 to 3
- conv_bias: float32 [5504], P('tp'), may hold values from -3 to 3
- down_weight: bfloat16 [5504, 2048], P('tp', 'fs'), may hold values from -0.078125 to 0.078125
Outputs:
- output: bfloat16 [12288, 2048], P(('fs', 'tp'))
All inputs are finite; a program needn't handle non-finite values.
Results may differ from a plain program's by a relative error of at most 0.012.
Values may be sent and summed in bfloat16 or wider, within the bound.
A program may use at most 128 MiB of HBM per device.

v0:
```python
import jax
import jax.numpy as jnp
from jax import lax
from jax.sharding import PartitionSpec as P

norm_eps = 1e-06


def body(
    mixed,
    residual,
    mix_weight,
    norm_gain,
    up_weight,
    gate_weight,
    conv_weight,
    conv_bias,
    down_weight,
):
    summed = jnp.dot(
        mixed,
        lax.all_gather(mix_weight, ("fs", "tp"), axis=0, tiled=True),
        preferred_element_type=jnp.float32,
    )
    stream = (residual.astype(jnp.float32) + summed).astype(jnp.bfloat16)
    x_float = stream.astype(jnp.float32)
    normed = (
        x_float
        * lax.rsqrt(jnp.mean(x_float * x_float, axis=-1, keepdims=True) + norm_eps)
        * norm_gain
    ).astype(jnp.bfloat16)
    half_cols = up_weight.shape[1]
    up_full, gate_full = (
        lax.all_gather(up_weight, "fs", axis=0, tiled=True),
        lax.all_gather(gate_weight, "fs", axis=0, tiled=True),
    )
    shard_piece = lax.all_gather(normed, "tp", axis=0, tiled=True)
    up_rows = jnp.dot(shard_piece, up_full, preferred_element_type=jnp.float32).astype(jnp.bfloat16)
    gate_rows = jnp.dot(shard_piece, gate_full, preferred_element_type=jnp.float32).astype(
        jnp.bfloat16
    )
    joined = jnp.concatenate([up_rows, gate_rows], axis=1)
    up_part = joined[:, :half_cols]
    gate_part = joined[:, half_cols:]
    up_float = lax.optimization_barrier(up_part).astype(jnp.float32)
    padded = jnp.pad(up_float, ((2, 0), (0, 0)))
    smoothed = (
        conv_bias
        + conv_weight[0] * padded[:-2]
        + conv_weight[1] * padded[1:-1]
        + conv_weight[2] * padded[2:]
    )
    hidden = (jax.nn.gelu(smoothed) * gate_part.astype(jnp.float32)).astype(jnp.bfloat16)
    down_full = lax.all_gather(down_weight, "fs", axis=1, tiled=True)
    summed_out = lax.psum_scatter(
        jnp.dot(hidden, down_full, preferred_element_type=jnp.float32).astype(jnp.bfloat16),
        "tp",
        scatter_dimension=0,
        tiled=True,
    ).astype(jnp.float32)
    return (x_float + summed_out).astype(jnp.bfloat16)


def solution(mesh):
    return jax.shard_map(
        body,
        mesh=mesh,
        in_specs=(
            P(("fs", "tp"), None),
            P(("fs", "tp"), None),
            P(("fs", "tp"), None),
            P(),
            P("fs", "tp"),
            P("fs", "tp"),
            P(None, "tp"),
            P("tp"),
            P("tp", "fs"),
        ),
        out_specs=P(("fs", "tp"), None),
        check_vma=False,
    )
```

profile of v0, /device:TPU:0, one launch (start us, length us, event | category | flops | bytes accessed | tf_op | source)
XLA Modules:
  0.0 495.7 jit_solution(2347268354048013400)
XLA Ops:
  6.5 0.0 copy-start
  6.5 0.0 all-gather.6.cloned.1.call-start
  6.5 0.7 all-gather.6.cloned.1.call-update
  7.3 0.0 all-gather.10.cloned.1.call-start
  7.3 0.7 all-gather.10.cloned.1.call-update
  8.0 0.0 copy-start.2
  8.0 0.0 all-gather.8.cloned.1.call-start
  8.1 81.9 %all-gather.6.cloned.1.call-done = bf16[2048,2048]{1,0:T(8,128)(2,1)} async-done(((bf16[64,2048]{1,0:T(8,128)(2,1)}), bf16[2048,2048]{1,0:T(8,128)(2,1)}) %all-gather.6.cloned.1.call-update) | async-done | bytes 8388624 | tf_op jit(solution)/shard_map/all_gather | solution.py:22
  90.0 0.0 copy-done
  90.0 7.4 %fusion.22 = (f32[384]{0:T(512)S(1)}, bf16[384,2048]{1,0:T(8,128)(2,1)S(1)}) fusion(bf16[384,2048]{1,0:T(8,128)(2,1)S(1)} %copy-done, bf16[2048,2048]{1,0:T(8,128)(2,1)} %all-gather.6.cloned.1.call-done, bf16[384,2048]{1,0:T(8,128)(2,1)} %param.10), kind=kOutput, calls=%fused_computation.31 | convolution fusion | flops 3225943552 | bytes 13108736 | tf_op jit(solution)/shard_map/dot_general | solution.py:20
  97.4 0.0 copy-start.1
  97.4 0.0 copy-done.2
  97.4 1.6 fusion.24
  99.0 0.0 all-gather.8.cloned.1.call-update
  99.0 0.0 all-gather.12.cloned.1.call-start
  99.0 0.5 all-gather.12.cloned.1.call-update
  99.6 0.0 all-gather.14.cloned.1.call-start
  99.6 0.5 all-gather.14.cloned.1.call-update
  100.2 0.2 reduce-scatter.2.cloned.1.call-start
  100.4 0.0 copy-done.1
  100.4 0.1 slice_reduce_fusion.2
  100.5 81.8 %all-gather.10.cloned.1.call-done = bf16[2048,1376]{0,1:T(8,128)(2,1)} async-done(((bf16[256,1376]{0,1:T(8,128)(2,1)}), bf16[2048,1376]{0,1:T(8,128)(2,1)}) %all-gather.10.cloned.1.call-update) | async-done | bytes 5636112 | tf_op jit(solution)/shard_map/all_gather | solution.py:34
  182.2 46.1 %all-gather.8.cloned.1.call-done = bf16[1536,2048]{1,0:T(8,128)(2,1)} async-done(((bf16[384,2048]{1,0:T(8,128)(2,1)}), bf16[1536,2048]{1,0:T(8,128)(2,1)}) %all-gather.8.cloned.1.call-update) | async-done | bytes 6291472 | tf_op jit(solution)/shard_map/all_gather | solution.py:37
  228.4 12.8 %convolution_convert_fusion.2 = bf16[1536,1376]{0,1:T(8,128)(2,1)S(1)} fusion(bf16[1536,2048]{1,0:T(8,128)(2,1)} %all-gather.8.cloned.1.call-done, bf16[2048,1376]{0,1:T(8,128)(2,1)} %all-gather.10.cloned.1.call-done), kind=kOutput, calls=%fused_computation.19 | convolution fusion | flops 8659156992 | bytes 16154624 | tf_op jit(solution)/shard_map/dot_general | solution.py:38
  241.2 0.0 copy-start.3
  241.2 4.5 convert_element_type.43
  245.7 76.1 %all-gather.12.cloned.1.call-done = bf16[2048,1376]{0,1:T(8,128)(2,1)} async-done(((bf16[256,1376]{0,1:T(8,128)(2,1)}), bf16[2048,1376]{0,1:T(8,128)(2,1)}) %all-gather.12.cloned.1.call-update) | async-done | bytes 5636112 | tf_op jit(solution)/shard_map/all_gather | solution.py:35
  321.9 0.0 copy-done.3
  321.9 21.8 %fusion.13.clone.4 = bf16[1536,1376]{0,1:T(8,128)(2,1)} fusion(f32[1536,1376]{0,1:T(8,128)} %convert_element_type.43, bf16[1536,2048]{1,0:T(8,128)(2,1)} %all-gather.8.cloned.1.call-done, bf16[2048,1376]{0,1:T(8,128)(2,1)} %all-gather.12.cloned.1.call-done, f32[1376]{0:T(1024)S(1)} %get-tuple-element.6, f32[1376]{0:T(1024)S(1)} %get-tuple-element.7, ...), kind=kOutput, calls=%fused_computation.16.clone.clone.clone.1 | convolution fusion | flops 8695087104 | bytes 24630784 | tf_op jit(solution)/shard_map/dot_general | solution.py:39
  343.6 69.9 %all-gather.14.cloned.1.call-done = bf16[1376,2048]{1,0:T(8,128)(2,1)} async-done(((bf16[1376,256]{1,0:T(8,128)(2,1)}), bf16[1376,2048]{1,0:T(8,128)(2,1)}) %all-gather.14.cloned.1.call-update) | async-done | bytes 5636112 | tf_op jit(solution)/shard_map/all_gather | solution.py:54
  413.5 15.0 %convolution_convert_fusion = bf16[1536,2048]{1,0:T(8,128)(2,1)} fusion(bf16[1376,2048]{1,0:T(8,128)(2,1)} %all-gather.14.cloned.1.call-done, bf16[1536,1376]{0,1:T(8,128)(2,1)} %fusion.13.clone.4), kind=kOutput, calls=%fused_computation.17 | convolution fusion | flops 8660189184 | bytes 16154624 | tf_op jit(solution)/shard_map/dot_general | solution.py:56
  428.5 0.0 reduce-scatter.2.cloned.1.call-update
  428.5 57.2 %reduce-scatter.2.cloned.1.call-done = bf16[384,2048]{1,0:T(8,128)(2,1)} async-done(((bf16[1536,2048]{1,0:T(8,128)(2,1)}), bf16[384,2048]{1,0:T(8,128)(2,1)}) %reduce-scatter.2.cloned.1.call-update) | async-done | bytes 1572880 | tf_op jit(solution)/shard_map/reduce_scatter | solution.py:55
  485.7 3.2 fusion.25
  (1 shorter events, 0.0 us)
Async XLA Ops:
  6.5 83.5 %copy-start = (bf16[384,2048]{1,0:T(8,128)(2,1)S(1)}, bf16[384,2048]{1,0:T(8,128)(2,1)}, u32[]{:S(2)}) copy-start(bf16[384,2048]{1,0:T(8,128)(2,1)} %param.9) | copy-start | bytes 4718596
  6.5 83.5 %all-gather.6.cloned.1.call-start = ((), (), s32[]{:S(2)}) async-start(), calls=%async_computation.1 | async-start | bytes 8650752 | tf_op jit(solution)/shard_map/all_gather | solution.py:22
  7.3 175.0 %all-gather.10.cloned.1.call-start = ((), (), s32[]{:S(2)}) async-start(), calls=%async_computation.3 | async-start | bytes 6340608 | tf_op jit(solution)/shard_map/all_gather | solution.py:34
  8.0 89.4 %copy-start.2 = (f32[2048]{0:T(1024)S(1)}, f32[2048]{0:T(1024)}, u32[]{:S(2)}) copy-start(f32[2048]{0:T(1024)} %param.12) | copy-start | bytes 24580
  8.0 220.4 %all-gather.8.cloned.1.call-start = ((), (), s32[]{:S(2)}) async-start(), calls=%async_computation.2 | async-start | bytes 7864320 | tf_op jit(solution)/shard_map/all_gather | solution.py:37
  97.4 3.0 copy-start.1
  99.0 222.9 %all-gather.12.cloned.1.call-start = ((), (), s32[]{:S(2)}) async-start(), calls=%async_computation.4 | async-start | bytes 6340608 | tf_op jit(solution)/shard_map/all_gather | solution.py:35
  99.6 313.9 %all-gather.14.cloned.1.call-start = ((), (), s32[]{:S(2)}) async-start(), calls=%async_computation.5 | async-start | bytes 6340608 | tf_op jit(solution)/shard_map/all_gather | solution.py:54
  100.2 385.5 %reduce-scatter.2.cloned.1.call-start = ((), (), s32[]{:S(2)}) async-start(), calls=%async_computation.6 | async-start | bytes 7864320 | tf_op jit(solution)/shard_map/reduce_scatter | solution.py:55
  241.2 80.7 %copy-start.3 = (f32[1376]{0:T(1024)S(1)}, f32[1376]{0:T(1024)}, u32[]{:S(2)}) copy-start(f32[1376]{0:T(1024)} %param.16) | copy-start | bytes 16516
Sparse Core Ops, SparseCore 0:
  10.2 79.7 all-gather.5
  92.0 90.1 all-gather.9
  183.8 44.5 all-gather.7
  230.3 91.5 all-gather.11
  323.7 89.7 all-gather.13
  428.6 57.0 reduce-scatter.1
where the time goes:
time: 496 us
  waiting for transfers between devices  416 us (84%)
  matrix products  56.9 us (11%)
  between operations  13.5 us (3%)
  other arithmetic  9.33 us (2%)
    all_gather x1, waiting for transfers between devices, body(): lax.all_gather(mix_weight, ('fs', 'tp'), axis=0, tiled=True)  81.9 us
    all_gather x1, waiting for transfers between devices, body(): lax.all_gather(up_weight, 'fs', axis=0, tiled=True)  81.8 us
    all_gather x1, waiting for transfers between devices, body(): lax.all_gather(gate_weight, 'fs', axis=0, tiled=True)  76.1 us
    all_gather x1, waiting for transfers between devices, body(): down_full = lax.all_gather(down_weight, 'fs', axis=1, tiled=True)  69.9 us
    reduce_scatter x1, waiting for transfers between devices, body(): lax.psum_scatter(jnp.dot(hidden, down_full, preferred_element_type=jnp.fl...  57.2 us
    all_gather x1, waiting for transfers between devices, body(): shard_piece = lax.all_gather(normed, 'tp', axis=0, tiled=True)  46.1 us
    dot_general x1, matrix products, body(): jnp.dot(shard_piece, gate_full, preferred_element_type=jnp.float32)  21.8 us
    dot_general x1, matrix products, body(): jnp.dot(hidden, down_full, preferred_element_type=jnp.float32)  15 us
  transfers between devices with their start and end apart: 6, of which 6 were waited for; matrix products, arithmetic and copies ran while one was open for 10% of the time, Pallas kernels for 0%

commit v1 on v0

--- a/solution.py
+++ b/solution.py
@@ -34,7 +34,12 @@
         lax.all_gather(up_weight, "fs", axis=0, tiled=True),
         lax.all_gather(gate_weight, "fs", axis=0, tiled=True),
     )
-    shard_piece = lax.all_gather(normed, "tp", axis=0, tiled=True)
+    ring = [normed]
+    for hop in range(3):
+        ring.append(lax.ppermute(ring[-1], "tp", [(dev, (dev + 1) % 4) for dev in range(4)]))
+    shard_piece = jnp.roll(
+        jnp.concatenate(ring[::-1], axis=0), (lax.axis_index("tp") + 1) * ring[0].shape[0], axis=0
+    )
     up_rows = jnp.dot(shard_piece, up_full, preferred_element_type=jnp.float32).astype(jnp.bfloat16)
     gate_rows = jnp.dot(shard_piece, gate_full, preferred_element_type=jnp.float32).astype(
         jnp.bfloat16

time: 496 us -> 448 us (0.903)
  waiting for transfers between devices: 416 us -> 352 us
  local copies, waits for them, and re-layouts: 0.07 us -> 13.8 us
    all_gather x1, waiting for transfers between devices: 81.8 us -> 7.46 us  [body(): lax.all_gather(up_weight, 'fs', axis=0, tiled=True)]
    ppermute x0 -> x3, waiting for transfers between devices: none -> 59.6 us  [body(): lax.ppermute(ring[-1], 'tp', [(dev, (dev + 1) % 4) for dev in range(4)])]
    all_gather x1 -> x0, waiting for transfers between devices: 46.1 us -> none  [body(): shard_piece = lax.all_gather(normed, 'tp', axis=0, tiled=True)]
    unnamed x8 -> x16, local copies, waits for them, and re-layouts: 0.02 us -> 13.8 us
  transfers between devices with their start and end apart: 6 -> 8, of which waited for: 6 -> 8; matrix products, arithmetic and copies ran while one was open for 10% -> 14% of each run, Pallas kernels for 0% -> 0%
where the time goes in v1:
time: 448 us
  waiting for transfers between devices  352 us (79%)
  matrix products  57.1 us (13%)
  local copies, waits for them, and re-layouts  13.8 us (3%)
  between operations  13.2 us (3%)
  other arithmetic  11.2 us (2%)
    all_gather x1, waiting for transfers between devices, body(): lax.all_gather(mix_weight, ('fs', 'tp'), axis=0, tiled=True)  81.2 us
    all_gather x1, waiting for transfers between devices, body(): lax.all_gather(gate_weight, 'fs', axis=0, tiled=True)  74.6 us
    all_gather x1, waiting for transfers between devices, body(): down_full = lax.all_gather(down_weight, 'fs', axis=1, tiled=True)  69.9 us
    ppermute x3, waiting for transfers between devices, body(): lax.ppermute(ring[-1], 'tp', [(dev, (dev + 1) % 4) for dev in range(4)])  59.6 us
    reduce_scatter x1, waiting for transfers between devices, body(): lax.psum_scatter(jnp.dot(hidden, down_full, preferred_element_type=jnp.fl...  57.2 us
    dot_general x1, matrix products, body(): jnp.dot(shard_piece, gate_full, preferred_element_type=jnp.float32)  21.8 us
    dot_general x1, matrix products, body(): jnp.dot(hidden, down_full, preferred_element_type=jnp.float32)  15.1 us
    unnamed x16, local copies, waits for them, and re-layouts  13.8 us
  transfers between devices with their start and end apart: 8, of which 8 were waited for; matrix products, arithmetic and copies ran while one was open for 14% of the time, Pallas kernels for 0%

profile of v1, /device:TPU:0, one launch (start us, length us, event | category | flops | bytes accessed | tf_op | source)
XLA Modules:
  0.0 447.8 jit_solution(4352930181993435649)
XLA Ops:
  6.5 0.0 copy-start
  6.5 0.0 all-gather.5.cloned.1.call-start
  6.5 0.7 all-gather.5.cloned.1.call-update
  7.3 0.0 all-gather.7.cloned.1.call-start
  7.3 0.7 all-gather.7.cloned.1.call-update
  8.0 0.0 all-gather.9.cloned.1.call-start
  8.1 0.7 all-gather.9.cloned.1.call-update
  8.7 0.0 copy-start.2
  8.8 0.0 copy-start.3
  8.8 0.0 all-gather.11.cloned.1.call-start
  8.8 81.2 %all-gather.5.cloned.1.call-done = bf16[2048,2048]{1,0:T(8,128)(2,1)} async-done(((bf16[64,2048]{1,0:T(8,128)(2,1)}), bf16[2048,2048]{1,0:T(8,128)(2,1)}) %all-gather.5.cloned.1.call-update) | async-done | bytes 8388624 | tf_op jit(solution)/shard_map/all_gather | solution.py:22
  90.0 0.0 copy-done
  90.0 7.4 %fusion.25 = (f32[384]{0:T(512)S(1)}, bf16[384,2048]{1,0:T(8,128)(2,1)S(1)}) fusion(bf16[384,2048]{1,0:T(8,128)(2,1)S(1)} %copy-done, bf16[2048,2048]{1,0:T(8,128)(2,1)} %all-gather.5.cloned.1.call-done, bf16[384,2048]{1,0:T(8,128)(2,1)} %param.10), kind=kOutput, calls=%fused_computation.33 | convolution fusion | flops 3225943552 | bytes 13108736 | tf_op jit(solution)/shard_map/dot_general | solution.py:20
  97.4 0.0 copy-done.2
  97.4 0.4 fusion.27
  97.8 0.3 collective-permute-start
  98.1 19.6 %collective-permute-done = bf16[384,2048]{1,0:T(8,128)(2,1)S(1)} collective-permute-done((bf16[384,2048]{1,0:T(8,128)(2,1)S(1)}, bf16[384,2048]{1,0:T(8,128)(2,1)S(1)}, u32[]{:S(2)}, u32[]{:S(2)}) %collective-permute-start) | collective-permute-done | bytes 1572896 | tf_op jit(solution)/shard_map/ppermute | solution.py:39
  117.7 0.0 collective-permute-start.1
  117.7 0.0 all-gather.11.cloned.1.call-update
  117.7 0.0 reduce-scatter.2.cloned.1.call-start
  117.8 19.9 %collective-permute-done.1 = bf16[384,2048]{1,0:T(8,128)(2,1)} collective-permute-done((bf16[384,2048]{1,0:T(8,128)(2,1)S(1)}, bf16[384,2048]{1,0:T(8,128)(2,1)}, u32[]{:S(2)}, u32[]{:S(2)}) %collective-permute-start.1) | collective-permute-done | bytes 1572896 | tf_op jit(solution)/shard_map/ppermute | solution.py:39
  137.7 0.0 collective-permute-start.2
  137.7 0.0 copy-done.3
  137.7 20.1 %collective-permute-done.2 = bf16[384,2048]{1,0:T(8,128)(2,1)} collective-permute-done((bf16[384,2048]{1,0:T(8,128)(2,1)}, bf16[384,2048]{1,0:T(8,128)(2,1)}, u32[]{:S(2)}, u32[]{:S(2)}) %collective-permute-start.2) | collective-permute-done | bytes 1572896 | tf_op jit(solution)/shard_map/ppermute | solution.py:39
  157.8 2.7 constant_dynamic-update-slice_fusion.7
  160.6 2.7 constant_dynamic-update-slice_fusion.6
  163.3 1.3 constant_dynamic-update-slice_fusion.5
  164.6 1.6 constant_dynamic-update-slice_fusion.4
  166.2 2.8 constant_dynamic-update-slice_fusion.3
  169.0 2.8 constant_dynamic-update-slice_fusion.2
  171.9 1.3 constant_dynamic-update-slice_fusion.1
  173.2 1.6 constant_dynamic-update-slice_fusion
  174.8 7.5 %all-gather.7.cloned.1.call-done = bf16[2048,1376]{0,1:T(8,128)(2,1)} async-done(((bf16[256,1376]{0,1:T(8,128)(2,1)}), bf16[2048,1376]{0,1:T(8,128)(2,1)}) %all-gather.7.cloned.1.call-update) | async-done | bytes 5636112 | tf_op jit(solution)/shard_map/all_gather | solution.py:34
  182.2 12.8 %convolution_convert_fusion.2 = bf16[1536,1376]{0,1:T(8,128)(2,1)S(1)} fusion(bf16[2048,1376]{0,1:T(8,128)(2,1)} %all-gather.7.cloned.1.call-done, bf16[3072,2048]{1,0:T(8,128)(2,1)} %constant_dynamic-update-slice_fusion, s32[]{:T(128)S(6)} %select_n.14), kind=kOutput, calls=%fused_computation.19 | convolution fusion | flops 8659156992 | bytes 16154628 | tf_op jit(solution)/shard_map/dot_general | solution.py:43
  195.0 0.0 copy-start.4
  195.0 4.4 convert_element_type.43
  199.4 74.6 %all-gather.9.cloned.1.call-done = bf16[2048,1376]{0,1:T(8,128)(2,1)} async-done(((bf16[256,1376]{0,1:T(8,128)(2,1)}), bf16[2048,1376]{0,1:T(8,128)(2,1)}) %all-gather.9.cloned.1.call-update) | async-done | bytes 5636112 | tf_op jit(solution)/shard_map/all_gather | solution.py:35
  274.1 0.0 copy-done.4
  274.1 21.8 %fusion.13.clone.4 = bf16[1536,1376]{0,1:T(8,128)(2,1)} fusion(f32[1536,1376]{0,1:T(8,128)} %convert_element_type.43, bf16[2048,1376]{0,1:T(8,128)(2,1)} %all-gather.9.cloned.1.call-done, bf16[3072,2048]{1,0:T(8,128)(2,1)} %constant_dynamic-update-slice_fusion, s32[]{:T(128)S(6)} %select_n.14, f32[1376]{0:T(1024)S(1)} %get-tuple-element.6, ...), kind=kOutput, calls=%fused_computation.16.clone.clone.clone.1 | convolution fusion | flops 8695087104 | bytes 24630788 | tf_op jit(solution)/shard_map/dot_general | solution.py:44
  295.8 69.9 %all-gather.11.cloned.1.call-done = bf16[1376,2048]{1,0:T(8,128)(2,1)} async-done(((bf16[1376,256]{1,0:T(8,128)(2,1)}), bf16[1376,2048]{1,0:T(8,128)(2,1)}) %all-gather.11.cloned.1.call-update) | async-done | bytes 5636112 | tf_op jit(solution)/shard_map/all_gather | solution.py:59
  365.7 0.0 copy-start.1
  365.7 15.1 %convolution_convert_fusion = bf16[1536,2048]{1,0:T(8,128)(2,1)} fusion(bf16[1376,2048]{1,0:T(8,128)(2,1)} %all-gather.11.cloned.1.call-done, bf16[1536,1376]{0,1:T(8,128)(2,1)} %fusion.13.clone.4), kind=kOutput, calls=%fused_computation.17 | convolution fusion | flops 8660189184 | bytes 16154624 | tf_op jit(solution)/shard_map/dot_general | solution.py:61
  380.8 0.0 reduce-scatter.2.cloned.1.call-update
  380.9 57.2 %reduce-scatter.2.cloned.1.call-done = bf16[384,2048]{1,0:T(8,128)(2,1)} async-done(((bf16[1536,2048]{1,0:T(8,128)(2,1)}), bf16[384,2048]{1,0:T(8,128)(2,1)}) %reduce-scatter.2.cloned.1.call-update) | async-done | bytes 1572880 | tf_op jit(solution)/shard_map/reduce_scatter | solution.py:60
  438.0 3.2 fusion.28
  441.3 0.0 copy-done.1
  (2 shorter events, 0.1 us)
Async XLA Ops:
  6.5 83.5 %copy-start = (bf16[384,2048]{1,0:T(8,128)(2,1)S(1)}, bf16[384,2048]{1,0:T(8,128)(2,1)}, u32[]{:S(2)}) copy-start(bf16[384,2048]{1,0:T(8,128)(2,1)} %param.9) | copy-start | bytes 4718596
  6.5 83.5 %all-gather.5.cloned.1.call-start = ((), (), s32[]{:S(2)}) async-start(), calls=%async_computation.1 | async-start | bytes 8650752 | tf_op jit(solution)/shard_map/all_gather | solution.py:22
  7.3 175.0 %all-gather.7.cloned.1.call-start = ((), (), s32[]{:S(2)}) async-start(), calls=%async_computation.2 | async-start | bytes 6340608 | tf_op jit(solution)/shard_map/all_gather | solution.py:34
  8.0 266.0 %all-gather.9.cloned.1.call-start = ((), (), s32[]{:S(2)}) async-start(), calls=%async_computation.3 | async-start | bytes 6340608 | tf_op jit(solution)/shard_map/all_gather | solution.py:35
  8.7 88.6 %copy-start.2 = (f32[2048]{0:T(1024)S(1)}, f32[2048]{0:T(1024)}, u32[]{:S(2)}) copy-start(f32[2048]{0:T(1024)} %param.12) | copy-start | bytes 24580
  8.8 128.9 %copy-start.3 = (f32[3,1376]{1,0:T(4,128)S(1)}, f32[3,1376]{1,0:T(4,128)}, u32[]{:S(2)}) copy-start(f32[3,1376]{1,0:T(4,128)} %param.15) | copy-start | bytes 49540
  8.8 357.0 %all-gather.11.cloned.1.call-start = ((), (), s32[]{:S(2)}) async-start(), calls=%async_computation.4 | async-start | bytes 6340608 | tf_op jit(solution)/shard_map/all_gather | solution.py:59
  97.8 19.9 %collective-permute-start = (bf16[384,2048]{1,0:T(8,128)(2,1)S(1)}, bf16[384,2048]{1,0:T(8,128)(2,1)S(1)}, u32[]{:S(2)}, u32[]{:S(2)}) collective-permute-start(bf16[384,2048]{1,0:T(8,128)(2,1)S(1)} %fusion.27), channel_id=1, source_target_pairs={{0,1},{1,2},{2,3},{3,0},{4,5},{5,6},{6,7},{7,4},{8,9},{9,10},{10,1... | collective-permute-start | bytes 4718600 | tf_op jit(solution)/shard_map/ppermute | solution.py:39
  117.7 19.9 %collective-permute-start.1 = (bf16[384,2048]{1,0:T(8,128)(2,1)S(1)}, bf16[384,2048]{1,0:T(8,128)(2,1)}, u32[]{:S(2)}, u32[]{:S(2)}) collective-permute-start(bf16[384,2048]{1,0:T(8,128)(2,1)S(1)} %collective-permute-done), channel_id=1, source_target_pairs={{0,1},{1,2},{2,3},{3,0},{4,5},{5,6},{6,7},{7,4},{8,9},{9,10},{10,1... | collective-permute-start | bytes 4718600 | tf_op jit(solution)/shard_map/ppermute | solution.py:39
  117.7 320.3 %reduce-scatter.2.cloned.1.call-start = ((), (), s32[]{:S(2)}) async-start(), calls=%async_computation.5 | async-start | bytes 7864320 | tf_op jit(solution)/shard_map/reduce_scatter | solution.py:60
  137.7 20.2 %collective-permute-start.2 = (bf16[384,2048]{1,0:T(8,128)(2,1)}, bf16[384,2048]{1,0:T(8,128)(2,1)}, u32[]{:S(2)}, u32[]{:S(2)}) collective-permute-start(bf16[384,2048]{1,0:T(8,128)(2,1)} %collective-permute-done.1), channel_id=1, source_target_pairs={{0,1},{1,2},{2,3},{3,0},{4,5},{5,6},{6,7},{7,4},{8,9},{9,10},{10,1... | collective-permute-start | bytes 4718600 | tf_op jit(solution)/shard_map/ppermute | solution.py:39
  195.0 79.0 %copy-start.4 = (f32[1376]{0:T(1024)S(1)}, f32[1376]{0:T(1024)}, u32[]{:S(2)}) copy-start(f32[1376]{0:T(1024)} %param.16) | copy-start | bytes 16516
  365.7 75.6 %copy-start.1 = (bf16[384,2048]{1,0:T(8,128)(2,1)S(1)}, bf16[384,2048]{1,0:T(8,128)(2,1)}, u32[]{:S(2)}) copy-start(bf16[384,2048]{1,0:T(8,128)(2,1)} %param.9) | copy-start | bytes 4718596
Sparse Core Ops, SparseCore 0:
  10.2 79.7 all-gather.4
  92.0 90.1 all-gather.6
  184.3 89.7 all-gather.8
  276.0 89.7 all-gather.10
  381.0 57.0 reduce-scatter.1
